TPU v7x, 32 devices: a whole 2x2x4 slice. The times are simulated.
32 devices in a mesh: grp: 2 (over y), fs: 4 (over z), tp: 4 (over x, core).
Axes of the slice: x: 2, y: 2, z: 4, core: 2. Of those that a mesh axis runs over, the one named last changes fastest.
Arguments:
- prompt: bfloat16 [2048, 2048], P(('grp', 'tp')), parts along dimension 0, may hold values from -6 to 6
- gain_first: float32 [2048], P('fs'), may hold values from 0.1 to 1.9
- gate_first: float32 [2048, 4096], P('fs', 'tp'), may hold values from -0.125 to 0.125
- up_first: float32 [2048, 4096], P('fs', 'tp'), may hold values from -0.125 to 0.125
- down_first: float32 [4096, 2048], P('fs', 'tp'), may hold values from -0.09375 to 0.09375
- gain_second: float32 [2048], P('fs'), may hold values from 0.1 to 1.9
- gate_second: float32 [2048, 4096], P('fs', 'tp'), may hold values from -0.125 to 0.125
- up_second: float32 [2048, 4096], P('fs', 'tp'), may hold values from -0.125 to 0.125
- down_second: float32 [4096, 2048], P('fs', 'tp'), may hold values from -0.09375 to 0.09375
Outputs:
- result: bfloat16 [2048, 2048], P(('grp', 'tp')), parts along dimension 0
- served_gate_first: bfloat16 [4096, 4096], P('grp', 'fs'), parts along dimension 0
- served_up_first: bfloat16 [4096, 4096], P('grp', 'fs'), parts along dimension 0
- served_down_first: bfloat16 [4096, 4096], P('fs', 'grp'), parts along dimension 1
- served_gate_second: bfloat16 [4096, 4096], P('grp', 'fs'), parts along dimension 0
- served_up_second: bfloat16 [4096, 4096], P('grp', 'fs'), parts along dimension 0
- served_down_second: bfloat16 [4096, 4096], P('fs', 'grp'), parts along dimension 1
There are 2 independent parts, one for each index of `grp`. A program takes and returns all parts, laid end to end along the dimension named above; an argument that names none is the same for every part. Nothing has to cross between parts.
All inputs are finite; a program needn't handle non-finite values.
Results may differ from a plain program's by a relative error of at most 0.0053.
Values may be sent and summed in bfloat16 or wider, within the bound.
A program may use at most 128 MiB of HBM per device.

v0:
```python
import jax
import jax.numpy as jnp
from jax import lax
from jax.sharding import PartitionSpec as P

EPS = 1e-06


def as_sent(array):
    return jax.tree.map(lambda a: a.astype(jnp.bfloat16) if a.dtype == jnp.float32 else a, array)


def fold(gain, weight):
    return (gain[:, None] * weight).astype(jnp.bfloat16)


def normed_of(stream):
    return (stream * lax.rsqrt(jnp.mean(stream * stream, axis=-1, keepdims=True) + EPS)).astype(
        jnp.bfloat16
    )


def hidden_of(normed, w_gate, w_up):
    gate = jnp.dot(normed, w_gate, preferred_element_type=jnp.float32)
    up_val = jnp.dot(normed, w_up, preferred_element_type=jnp.float32)
    return (jax.nn.silu(gate) * up_val).astype(jnp.bfloat16)


def on_device(
    prompt,
    gain_first,
    gate_first,
    up_first,
    down_first,
    gain_second,
    gate_second,
    up_second,
    down_second,
):
    folded = (
        fold(gain_first, gate_first),
        fold(gain_first, up_first),
        fold(gain_second, gate_second),
        fold(gain_second, up_second),
    )
    downs = (down_first.astype(jnp.bfloat16), down_second.astype(jnp.bfloat16))
    spread = (
        lax.all_to_all(folded[0], "tp", split_axis=0, concat_axis=1, tiled=True),
        lax.all_to_all(folded[1], "tp", split_axis=0, concat_axis=1, tiled=True),
        lax.all_to_all(folded[2], "tp", split_axis=0, concat_axis=1, tiled=True),
        lax.all_to_all(folded[3], "tp", split_axis=0, concat_axis=1, tiled=True),
    )
    moved = (
        lax.all_to_all(spread[0], "fs", split_axis=1, concat_axis=0, tiled=True),
        lax.all_to_all(spread[1], "fs", split_axis=1, concat_axis=0, tiled=True),
        lax.all_to_all(spread[2], "fs", split_axis=1, concat_axis=0, tiled=True),
        lax.all_to_all(spread[3], "fs", split_axis=1, concat_axis=0, tiled=True),
    )
    n_fs = lax.axis_size("fs")
    width = moved[0].shape[1]
    piece = moved[0].shape[0] // n_fs
    shaped = tuple((m.reshape(n_fs, piece, width) for m in moved))
    joined = jax.tree.map(
        lambda part, own: part.astype(own.dtype),
        lax.all_gather(as_sent(shaped), "tp", axis=1, tiled=True),
        shaped,
    )
    served = tuple((m.reshape(-1, width) for m in joined))
    served_downs = (
        lax.all_gather(downs[0], "tp", axis=1, tiled=True),
        lax.all_gather(downs[1], "tp", axis=1, tiled=True),
    )
    gates = (served[0], served[2])
    ups = (served[1], served[3])
    stream = prompt.astype(jnp.float32)
    for layer in range(2):
        hidden = hidden_of(normed_of(stream), gates[layer], ups[layer])
        partial_out = jnp.dot(hidden, served_downs[layer], preferred_element_type=jnp.float32)
        stream = stream + 0.5 * lax.psum(partial_out, "fs")
    result = stream.astype(jnp.bfloat16)
    return (result, served[0], served[1], served_downs[0], served[2], served[3], served_downs[1])


def solution(mesh):
    return jax.shard_map(
        on_device,
        mesh=mesh,
        in_specs=(
            P(("grp", "tp"), None),
            P("fs"),
            P("fs", "tp"),
            P("fs", "tp"),
            P("fs", "tp"),
            P("fs"),
            P("fs", "tp"),
            P("fs", "tp"),
            P("fs", "tp"),
        ),
        out_specs=(
            P(("grp", "tp"), None),
            P("grp", "fs"),
            P("grp", "fs"),
            P("fs", "grp"),
            P("grp", "fs"),
            P("grp", "fs"),
            P("fs", "grp"),
        ),
        check_vma=False,
    )
```

profile of v0, /device:TPU:0, one launch (start us, length us, event | category | flops | bytes accessed | tf_op | source)
XLA Modules:
  0.0 552.0 jit_solution(7371921522746309)
XLA Ops:
  7.2 2.5 multiply_convert_fusion.4
  9.7 18.5 %all_to_all.116 = bf16[4,128,1024]{2,1,0:T(8,128)(2,1)S(1)} all-to-all(bf16[4,128,1024]{2,1,0:T(8,128)(2,1)S(1)} %bitcast.43), channel_id=1, replica_groups=mesh['grp'=2,'fs'=4,'tp'=4] {'tp'}, dimensions={0} | all-to-all | bytes 2097152 | tf_op jit(solution)/shard_map/all_to_all | solution.py:48
  28.2 30.1 %all_to_all.117 = bf16[128,4,1024]{2,0,1:T(8,128)(2,1)} all-to-all(bf16[128,4,1024]{2,0,1:T(8,128)(2,1)S(1)} %bitcast.37), channel_id=1, replica_groups=mesh['grp'=2,'fs'=4,'tp'=4] {'fs'}, dimensions={1} | all-to-all | bytes 2097152 | tf_op jit(solution)/shard_map/all_to_all | solution.py:54
  58.4 2.7 convert_element_type.41
  61.2 28.0 %all_to_all.118 = bf16[4,128,1024]{2,1,0:T(8,128)(2,1)S(1)} all-to-all(bf16[4,128,1024]{2,1,0:T(8,128)(2,1)S(1)} %bitcast.42), channel_id=1, replica_groups=mesh['grp'=2,'fs'=4,'tp'=4] {'tp'}, dimensions={0} | all-to-all | bytes 2097152 | tf_op jit(solution)/shard_map/all_to_all | solution.py:49
  89.2 28.6 %all_to_all.119 = bf16[128,4,1024]{2,0,1:T(8,128)(2,1)} all-to-all(bf16[128,4,1024]{2,0,1:T(8,128)(2,1)S(1)} %bitcast.38), channel_id=1, replica_groups=mesh['grp'=2,'fs'=4,'tp'=4] {'fs'}, dimensions={1} | all-to-all | bytes 2097152 | tf_op jit(solution)/shard_map/all_to_all | solution.py:55
  117.9 3.5 multiply_convert_fusion.1
  121.4 3.6 all-to-all-start.4
  125.4 4.5 fusion.10
  129.9 14.3 %all-gather.11.cloned.1.call-done = bf16[1024,2048]{1,0:T(8,128)(2,1)} async-done(((bf16[1024,512]{1,0:T(8,128)(2,1)}), bf16[1024,2048]{1,0:T(8,128)(2,1)}) %all-gather.11.cloned.1.call-update) | async-done | bytes 4194320 | tf_op jit(solution)/shard_map/all_gather | solution.py:70
  144.1 38.1 %all-gather.9.cloned.1.call-done = bf16[4,512,1024]{2,1,0:T(8,128)(2,1)} async-done(((bf16[4,128,1024]{2,1,0:T(8,128)(2,1)}), bf16[4,512,1024]{2,1,0:T(8,128)(2,1)}) %all-gather.9.cloned.1.call-update) | async-done | bytes 4194320 | tf_op jit(solution)/shard_map/all_gather | solution.py:65
  182.2 7.6 %fusion.5 = f32[256,2048]{1,0:T(8,128)} fusion(bf16[1024,2048]{1,0:T(8,128)(2,1)} %all-gather.11.cloned.1.call-done, bf16[2048,1024]{1,0:T(8,128)(2,1)} %bitcast.26, f32[256,1024]{1,0:T(8,128)} %fusion.10, bf16[256,2048]{1,0:T(8,128)(2,1)S(1)} %copy-done.1, f32[256]{0:T(256)S(1)} %add_rsqrt_fusion.1), kind=kOutput, calls=%fused_computation.17 | convolution fusion | flops 2150629376 | bytes 12583936 | tf_op jit(solution)/shard_map/dot_general | solution.py:78
  189.9 57.0 %all_to_all.120 = bf16[128,4,1024]{2,0,1:T(8,128)(2,1)} all-to-all(bf16[128,4,1024]{2,0,1:T(8,128)(2,1)S(1)} %bitcast.34), channel_id=1, replica_groups=mesh['grp'=2,'fs'=4,'tp'=4] {'fs'}, dimensions={1} | all-to-all | bytes 2097152 | tf_op jit(solution)/shard_map/all_to_all | solution.py:56
  247.0 2.7 convert_element_type.46
  249.8 16.9 %all_to_all.121 = bf16[4,128,1024]{2,1,0:T(8,128)(2,1)S(1)} all-to-all(bf16[4,128,1024]{2,1,0:T(8,128)(2,1)S(1)} %bitcast.40), channel_id=1, replica_groups=mesh['grp'=2,'fs'=4,'tp'=4] {'tp'}, dimensions={0} | all-to-all | bytes 2097152 | tf_op jit(solution)/shard_map/all_to_all | solution.py:51
  266.6 52.7 %all_to_all.122 = bf16[128,4,1024]{2,0,1:T(8,128)(2,1)} all-to-all(bf16[128,4,1024]{2,0,1:T(8,128)(2,1)S(1)} %bitcast.39), channel_id=1, replica_groups=mesh['grp'=2,'fs'=4,'tp'=4] {'fs'}, dimensions={1} | all-to-all | bytes 2097152 | tf_op jit(solution)/shard_map/all_to_all | solution.py:57
  319.9 2.2 multiply_reduce_fusion
  323.4 31.3 %all-gather.13.cloned.1.call-done = bf16[4,512,1024]{2,1,0:T(8,128)(2,1)} async-done(((bf16[4,128,1024]{2,1,0:T(8,128)(2,1)}), bf16[4,512,1024]{2,1,0:T(8,128)(2,1)}) %all-gather.13.cloned.1.call-update) | async-done | bytes 4194320 | tf_op jit(solution)/shard_map/all_gather | solution.py:65
  354.7 4.7 fusion.14
  359.4 31.7 %all-gather.17.cloned.1.call-done = bf16[1024,2048]{1,0:T(8,128)(2,1)} async-done(((bf16[1024,512]{1,0:T(8,128)(2,1)}), bf16[1024,2048]{1,0:T(8,128)(2,1)}) %all-gather.17.cloned.1.call-update) | async-done | bytes 4194320 | tf_op jit(solution)/shard_map/all_gather | solution.py:71
  391.2 36.0 %all-gather.15.cloned.1.call-done = bf16[4,512,1024]{2,1,0:T(8,128)(2,1)} async-done(((bf16[4,128,1024]{2,1,0:T(8,128)(2,1)}), bf16[4,512,1024]{2,1,0:T(8,128)(2,1)}) %all-gather.15.cloned.1.call-update) | async-done | bytes 4194320 | tf_op jit(solution)/shard_map/all_gather | solution.py:65
  427.2 7.9 %fusion.4 = f32[256,2048]{1,0:T(8,128)} fusion(bf16[1024,2048]{1,0:T(8,128)(2,1)} %all-gather.17.cloned.1.call-done, bf16[256,2048]{1,0:T(8,128)(2,1)} %multiply_convert_fusion.2, bf16[2048,1024]{1,0:T(8,128)(2,1)} %bitcast.30, f32[256,1024]{1,0:T(8,128)} %fusion.14), kind=kOutput, calls=%fused_computation.16 | convolution fusion | flops 2149056512 | bytes 12582912 | tf_op jit(solution)/shard_map/dot_general | solution.py:78
  435.1 86.3 %all-reduce.5.cloned.1.call-done = f32[256,2048]{1,0:T(8,128)} async-done(((f32[256,2048]{1,0:T(8,128)}), f32[256,2048]{1,0:T(8,128)}) %all-reduce.5.cloned.1.call-update) | async-done | bytes 2097168 | tf_op jit(solution)/shard_map/psum | solution.py:79
  521.4 3.2 add_convert_fusion
  (47 shorter events, 23.1 us)
Async XLA Ops:
  7.2 118.2 %all-gather.7.cloned.1.call-start = ((), (), s32[]{:S(2)}) async-start(), calls=%async_computation.8 | async-start | bytes 5242880 | tf_op jit(solution)/shard_map/all_gather | solution.py:65
  58.4 85.8 %all-gather.11.cloned.1.call-start = ((), (), s32[]{:S(2)}) async-start(), calls=%async_computation.10 | async-start | bytes 5242880 | tf_op jit(solution)/shard_map/all_gather | solution.py:70
  61.1 121.1 %all-gather.9.cloned.1.call-start = ((), (), s32[]{:S(2)}) async-start(), calls=%async_computation.9 | async-start | bytes 5242880 | tf_op jit(solution)/shard_map/all_gather | solution.py:65
  89.2 28.6 %copy-start.8 = (f32[512]{0:T(512)S(1)}, f32[512]{0:T(512)}, u32[]{:S(2)}) copy-start(f32[512]{0:T(512)} %param.14) | copy-start | bytes 6148
  121.4 3.7 copy-start.1
  121.4 68.6 %all-to-all-start.4 = ((bf16[4,128,1024]{2,1,0:T(8,128)(2,1)}), bf16[4,128,1024]{2,1,0:T(8,128)(2,1)S(1)}, u32[]{:S(2)}, u32[]{:S(2)}) async-start(bf16[4,128,1024]{2,1,0:T(8,128)(2,1)} %bitcast.41), calls=%async_computation.4 | async-start | bytes 2097152 | tf_op jit(solution)/shard_map/all_to_all | solution.py:50
  125.0 194.8 %all-reduce.3.cloned.1.call-start = ((), (), s32[]{:S(2)}) async-start(), calls=%async_computation.11 | async-start | bytes 4194304 | tf_op jit(solution)/shard_map/psum | solution.py:79
  189.9 164.8 %all-gather.13.cloned.1.call-start = ((), (), s32[]{:S(2)}) async-start(), calls=%async_computation.12 | async-start | bytes 5242880 | tf_op jit(solution)/shard_map/all_gather | solution.py:65
  246.9 144.2 %all-gather.17.cloned.1.call-start = ((), (), s32[]{:S(2)}) async-start(), calls=%async_computation.14 | async-start | bytes 5242880 | tf_op jit(solution)/shard_map/all_gather | solution.py:71
  249.7 177.5 %all-gather.15.cloned.1.call-start = ((), (), s32[]{:S(2)}) async-start(), calls=%async_computation.13 | async-start | bytes 5242880 | tf_op jit(solution)/shard_map/all_gather | solution.py:65
  319.3 202.1 %all-reduce.5.cloned.1.call-start = ((), (), s32[]{:S(2)}) async-start(), calls=%async_computation.15 | async-start | bytes 4194304 | tf_op jit(solution)/shard_map/psum | solution.py:79
  319.9 2.2 copy-start
  521.4 3.2 copy-start.2
  524.6 3.7 copy-start.4
  528.3 3.7 copy-start.3
  532.0 3.7 copy-start.5
  535.7 3.7 copy-start.7
  539.4 3.7 copy-start.6
Sparse Core Ops, SparseCore 0:
  58.5 43.5 all-gather.6
  104.3 39.8 all-gather.10
  145.7 36.5 all-gather.8
  190.0 129.8 all-reduce.2
  321.3 33.3 all-gather.12
  356.7 34.4 all-gather.16
  392.7 34.4 all-gather.14
  435.2 86.1 all-reduce.4
where the time goes:
time: 553 us; the launch traced here: 552 us
  waiting for transfers between devices  238 us (43%)
  blocking collectives  232 us (42%)
  matrix products  24.7 us (4%)
  local copies, waits for them, and re-layouts  20.6 us (4%)
  other arithmetic  18.4 us (3%)
  between operations  14.2 us (3%)
    all_gather x4, waiting for transfers between devices, on_device(): lax.all_gather(as_sent(shaped), 'tp', axis=1, tiled=True)  106 us
    psum x2, waiting for transfers between devices, on_device(): stream = stream + 0.5 * lax.psum(partial_out, 'fs')  86.8 us
    all_to_all x1, blocking collectives, on_device(): lax.all_to_all(spread[2], 'fs', split_axis=1, concat_axis=0, tiled=True)  57 us
    all_to_all x1, blocking collectives, on_device(): lax.all_to_all(spread[3], 'fs', split_axis=1, concat_axis=0, tiled=True)  52.7 us
    all_gather x1, waiting for transfers between devices, on_device(): lax.all_gather(downs[1], 'tp', axis=1, tiled=True)  31.7 us
    all_to_all x1, blocking collectives, on_device(): lax.all_to_all(spread[0], 'fs', split_axis=1, concat_axis=0, tiled=True)  30.1 us
    all_to_all x1, blocking collectives, on_device(): lax.all_to_all(spread[1], 'fs', split_axis=1, concat_axis=0, tiled=True)  28.6 us
    all_to_all x1, blocking collectives, on_device(): lax.all_to_all(folded[1], 'tp', split_axis=0, concat_axis=1, tiled=True)  28 us
  transfers between devices with their start and end apart: 9, of which 7 were waited for; matrix products, arithmetic and copies ran while one was open for 5% of the time, Pallas kernels for 0%

commit v1 on v0

--- a/solution.py
+++ b/solution.py
@@ -4,6 +4,11 @@
 from jax.sharding import PartitionSpec as P
 
 EPS = 1e-06
+
+
+def summed_here(x, name):
+    parts = lax.all_gather(x, name)
+    return jnp.sum(parts, axis=0)
 
 
 def as_sent(array):
@@ -76,7 +81,7 @@
     for layer in range(2):
         hidden = hidden_of(normed_of(stream), gates[layer], ups[layer])
         partial_out = jnp.dot(hidden, served_downs[layer], preferred_element_type=jnp.float32)
-        stream = stream + 0.5 * lax.psum(partial_out, "fs")
+        stream = stream + 0.5 * summed_here(partial_out, "fs")
     result = stream.astype(jnp.bfloat16)
     return (result, served[0], served[1], served_downs[0], served[2], served[3], served_downs[1])
 

time: 553 us -> 675 us (1.22)
  waiting for transfers between devices: 238 us -> 333 us
  blocking collectives: 232 us -> 257 us
    all_gather x0 -> x2, waiting for transfers between devices: none -> 184 us  [summed_here(): parts = lax.all_gather(x, name)]
    psum x2 -> x0, waiting for transfers between devices: 86.8 us -> none  [on_device(): stream = stream + 0.5 * lax.psum(partial_out, 'fs')]
    all_to_all x0 -> x1, blocking collectives: none -> 16.9 us  [on_device(): lax.all_to_all(folded[2], 'tp', split_axis=0, concat_axis=1, tiled=True)]
    reduce_sum x0 -> x2, other arithmetic: none -> 10.1 us  [summed_here(): return jnp.sum(parts, axis=0)]
  transfers between devices with their start and end apart: 9 -> 8, of which waited for: 7 -> 7; matrix products, arithmetic and copies ran while one was open for 5% -> 3% of each run, Pallas kernels for 0% -> 0%
where the time goes in v1:
time: 675 us; the launch traced here: 674 us
  waiting for transfers between devices  333 us (49%)
  blocking collectives  257 us (38%)
  other arithmetic  24.2 us (4%)
  matrix products  23.4 us (3%)
  local copies, waits for them, and re-layouts  21.1 us (3%)
  between operations  14.2 us (2%)
    all_gather x2, waiting for transfers between devices, summed_here(): parts = lax.all_gather(x, name)  184 us
    all_gather x4, waiting for transfers between devices, on_device(): lax.all_gather(as_sent(shaped), 'tp', axis=1, tiled=True)  100 us
    all_to_all x1, blocking collectives, on_device(): lax.all_to_all(spread[2], 'fs', split_axis=1, concat_axis=0, tiled=True)  61.6 us
    all_to_all x1, blocking collectives, on_device(): lax.all_to_all(spread[3], 'fs', split_axis=1, concat_axis=0, tiled=True)  58 us
    all_gather x1, waiting for transfers between devices, on_device(): lax.all_gather(downs[1], 'tp', axis=1, tiled=True)  31.7 us
    all_to_all x1, blocking collectives, on_device(): lax.all_to_all(spread[0], 'fs', split_axis=1, concat_axis=0, tiled=True)  30.3 us
    all_to_all x1, blocking collectives, on_device(): lax.all_to_all(spread[1], 'fs', split_axis=1, concat_axis=0, tiled=True)  28.6 us
    all_to_all x1, blocking collectives, on_device(): lax.all_to_all(folded[1], 'tp', split_axis=0, concat_axis=1, tiled=True)  26.5 us
  transfers between devices with their start and end apart: 8, of which 7 were waited for; matrix products, arithmetic and copies ran while one was open for 3% of the time, Pallas kernels for 0%

profile of v1, /device:TPU:0, one launch (start us, length us, event | category | flops | bytes accessed | tf_op | source)
XLA Modules:
  0.0 673.9 jit_solution(2388162379954160333)
XLA Ops:
  7.2 2.5 multiply_convert_fusion.4
  9.7 18.5 %all_to_all.116 = bf16[4,128,1024]{2,1,0:T(8,128)(2,1)S(1)} all-to-all(bf16[4,128,1024]{2,1,0:T(8,128)(2,1)S(1)} %bitcast.46), channel_id=1, replica_groups=mesh['grp'=2,'fs'=4,'tp'=4] {'tp'}, dimensions={0} | all-to-all | bytes 2097152 | tf_op jit(solution)/shard_map/all_to_all | solution.py:53
  28.2 30.3 %all_to_all.117 = bf16[128,4,1024]{2,0,1:T(8,128)(2,1)} all-to-all(bf16[128,4,1024]{2,0,1:T(8,128)(2,1)S(1)} %bitcast.40), channel_id=1, replica_groups=mesh['grp'=2,'fs'=4,'tp'=4] {'fs'}, dimensions={1} | all-to-all | bytes 2097152 | tf_op jit(solution)/shard_map/all_to_all | solution.py:59
  59.7 26.5 %all_to_all.118 = bf16[4,128,1024]{2,1,0:T(8,128)(2,1)S(1)} all-to-all(bf16[4,128,1024]{2,1,0:T(8,128)(2,1)S(1)} %bitcast.44), channel_id=1, replica_groups=mesh['grp'=2,'fs'=4,'tp'=4] {'tp'}, dimensions={0} | all-to-all | bytes 2097152 | tf_op jit(solution)/shard_map/all_to_all | solution.py:54
  86.2 28.6 %all_to_all.119 = bf16[128,4,1024]{2,0,1:T(8,128)(2,1)} all-to-all(bf16[128,4,1024]{2,0,1:T(8,128)(2,1)S(1)} %bitcast.41), channel_id=1, replica_groups=mesh['grp'=2,'fs'=4,'tp'=4] {'fs'}, dimensions={1} | all-to-all | bytes 2097152 | tf_op jit(solution)/shard_map/all_to_all | solution.py:60
  115.2 3.5 fusion.10
  118.7 16.8 %all-gather.15.cloned.1.call-done = bf16[1024,2048]{1,0:T(8,128)(2,1)} async-done(((bf16[1024,512]{1,0:T(8,128)(2,1)}), bf16[1024,2048]{1,0:T(8,128)(2,1)}) %all-gather.15.cloned.1.call-update) | async-done | bytes 4194320 | tf_op jit(solution)/shard_map/all_gather | solution.py:75
  135.5 36.1 %all-gather.13.cloned.1.call-done = bf16[4,512,1024]{2,1,0:T(8,128)(2,1)} async-done(((bf16[4,128,1024]{2,1,0:T(8,128)(2,1)}), bf16[4,512,1024]{2,1,0:T(8,128)(2,1)}) %all-gather.13.cloned.1.call-update) | async-done | bytes 4194320 | tf_op jit(solution)/shard_map/all_gather | solution.py:70
  171.5 7.4 %fusion.5 = f32[256,2048]{1,0:T(8,128)} fusion(bf16[1024,2048]{1,0:T(8,128)(2,1)} %all-gather.15.cloned.1.call-done, bf16[2048,1024]{1,0:T(8,128)(2,1)} %bitcast.30, f32[256,1024]{1,0:T(8,128)S(1)} %fusion.10, bf16[256,2048]{1,0:T(8,128)(2,1)S(1)} %copy-done, f32[256]{0:T(256)S(1)} %add_rsqrt_fusion.1), kind=kOutput, calls=%fused_computation.17 | convolution fusion | flops 2150629376 | bytes 12583936 | tf_op jit(solution)/shard_map/dot_general | solution.py:83
  182.1 16.9 %all_to_all.120 = bf16[4,128,1024]{2,1,0:T(8,128)(2,1)S(1)} all-to-all(bf16[4,128,1024]{2,1,0:T(8,128)(2,1)S(1)} %bitcast.47), channel_id=1, replica_groups=mesh['grp'=2,'fs'=4,'tp'=4] {'tp'}, dimensions={0} | all-to-all | bytes 2097152 | tf_op jit(solution)/shard_map/all_to_all | solution.py:55
  199.0 61.6 %all_to_all.121 = bf16[128,4,1024]{2,0,1:T(8,128)(2,1)} all-to-all(bf16[128,4,1024]{2,0,1:T(8,128)(2,1)S(1)} %bitcast.42), channel_id=1, replica_groups=mesh['grp'=2,'fs'=4,'tp'=4] {'fs'}, dimensions={1} | all-to-all | bytes 2097152 | tf_op jit(solution)/shard_map/all_to_all | solution.py:61
  260.7 2.7 convert_element_type.46
  263.4 17.0 %all_to_all.122 = bf16[4,128,1024]{2,1,0:T(8,128)(2,1)S(1)} all-to-all(bf16[4,128,1024]{2,1,0:T(8,128)(2,1)S(1)} %bitcast.45), channel_id=1, replica_groups=mesh['grp'=2,'fs'=4,'tp'=4] {'tp'}, dimensions={0} | all-to-all | bytes 2097152 | tf_op jit(solution)/shard_map/all_to_all | solution.py:56
  280.4 58.0 %all_to_all.123 = bf16[128,4,1024]{2,0,1:T(8,128)(2,1)} all-to-all(bf16[128,4,1024]{2,0,1:T(8,128)(2,1)S(1)} %bitcast.43), channel_id=1, replica_groups=mesh['grp'=2,'fs'=4,'tp'=4] {'fs'}, dimensions={1} | all-to-all | bytes 2097152 | tf_op jit(solution)/shard_map/all_to_all | solution.py:62
  338.7 34.7 %all-gather.23.cloned.1.call-done = f32[1024,2048]{1,0:T(8,128)} async-done(((f32[256,2048]{1,0:T(8,128)}), f32[1024,2048]{1,0:T(8,128)}) %all-gather.23.cloned.1.call-update) | async-done | bytes 8388624 | tf_op jit(solution)/shard_map/all_gather | solution.py:10
  373.3 4.4 reduce_sum.37
  379.5 27.9 %all-gather.17.cloned.1.call-done = bf16[4,512,1024]{2,1,0:T(8,128)(2,1)} async-done(((bf16[4,128,1024]{2,1,0:T(8,128)(2,1)}), bf16[4,512,1024]{2,1,0:T(8,128)(2,1)}) %all-gather.17.cloned.1.call-update) | async-done | bytes 4194320 | tf_op jit(solution)/shard_map/all_gather | solution.py:70
  407.4 4.7 fusion.14
  412.1 31.7 %all-gather.21.cloned.1.call-done = bf16[1024,2048]{1,0:T(8,128)(2,1)} async-done(((bf16[1024,512]{1,0:T(8,128)(2,1)}), bf16[1024,2048]{1,0:T(8,128)(2,1)}) %all-gather.21.cloned.1.call-update) | async-done | bytes 4194320 | tf_op jit(solution)/shard_map/all_gather | solution.py:76
  443.9 36.0 %all-gather.19.cloned.1.call-done = bf16[4,512,1024]{2,1,0:T(8,128)(2,1)} async-done(((bf16[4,128,1024]{2,1,0:T(8,128)(2,1)}), bf16[4,512,1024]{2,1,0:T(8,128)(2,1)}) %all-gather.19.cloned.1.call-update) | async-done | bytes 4194320 | tf_op jit(solution)/shard_map/all_gather | solution.py:70
  479.9 7.9 %fusion.4 = f32[256,2048]{1,0:T(8,128)} fusion(bf16[1024,2048]{1,0:T(8,128)(2,1)} %all-gather.21.cloned.1.call-done, bf16[256,2048]{1,0:T(8,128)(2,1)} %multiply_convert_fusion.2, bf16[2048,1024]{1,0:T(8,128)(2,1)} %bitcast.34, f32[256,1024]{1,0:T(8,128)} %fusion.14), kind=kOutput, calls=%fused_computation.16 | convolution fusion | flops 2149056512 | bytes 12582912 | tf_op jit(solution)/shard_map/dot_general | solution.py:83
  487.8 149.8 %all-gather.25.cloned.1.call-done = f32[1024,2048]{1,0:T(8,128)} async-done(((f32[256,2048]{1,0:T(8,128)}), f32[1024,2048]{1,0:T(8,128)}) %all-gather.25.cloned.1.call-update) | async-done | bytes 8388624 | tf_op jit(solution)/shard_map/all_gather | solution.py:10
  637.6 5.7 reduce_sum.39
  643.3 3.2 add_convert_fusion
  (48 shorter events, 27.4 us)
Async XLA Ops:
  7.2 108.0 %all-gather.11.cloned.1.call-start = ((), (), s32[]{:S(2)}) async-start(), calls=%async_computation.8 | async-start | bytes 5242880 | tf_op jit(solution)/shard_map/all_gather | solution.py:70
  28.2 30.3 %copy-start.7 = (f32[1024,512]{1,0:T(8,128)S(1)}, f32[1024,512]{1,0:T(8,128)}, u32[]{:S(2)}) copy-start(f32[1024,512]{1,0:T(8,128)} %param.13) | copy-start | bytes 6291460
  58.5 77.0 %all-gather.15.cloned.1.call-start = ((), (), s32[]{:S(2)}) async-start(), calls=%async_computation.10 | async-start | bytes 5242880 | tf_op jit(solution)/shard_map/all_gather | solution.py:75
  59.7 111.8 %all-gather.13.cloned.1.call-start = ((), (), s32[]{:S(2)}) async-start(), calls=%async_computation.9 | async-start | bytes 5242880 | tf_op jit(solution)/shard_map/all_gather | solution.py:70
  86.2 28.7 %copy-start = (bf16[256,2048]{1,0:T(8,128)(2,1)S(1)}, bf16[256,2048]{1,0:T(8,128)(2,1)}, u32[]{:S(2)}) copy-start(bf16[256,2048]{1,0:T(8,128)(2,1)} %param.9) | copy-start | bytes 3145732
  114.8 258.5 %all-gather.23.cloned.1.call-start = ((), (), s32[]{:S(2)}) async-start(), calls=%async_computation.14 | async-start | bytes 10485760 | tf_op jit(solution)/shard_map/all_gather | solution.py:10
  178.9 0.7 copy-start.8
  178.9 228.4 %all-gather.17.cloned.1.call-start = ((), (), s32[]{:S(2)}) async-start(), calls=%async_computation.11 | async-start | bytes 5242880 | tf_op jit(solution)/shard_map/all_gather | solution.py:70
  260.6 183.3 %all-gather.21.cloned.1.call-start = ((), (), s32[]{:S(2)}) async-start(), calls=%async_computation.13 | async-start | bytes 5242880 | tf_op jit(solution)/shard_map/all_gather | solution.py:76
  263.4 216.5 %all-gather.19.cloned.1.call-start = ((), (), s32[]{:S(2)}) async-start(), calls=%async_computation.12 | async-start | bytes 5242880 | tf_op jit(solution)/shard_map/all_gather | solution.py:70
  338.4 299.1 %all-gather.25.cloned.1.call-start = ((), (), s32[]{:S(2)}) async-start(), calls=%async_computation.15 | async-start | bytes 10485760 | tf_op jit(solution)/shard_map/all_gather | solution.py:10
  643.3 3.2 copy-start.1
  646.5 3.7 copy-start.3
  650.2 3.7 copy-start.2
  653.9 3.7 copy-start.4
  657.6 3.7 copy-start.6
  661.3 3.7 copy-start.5
Sparse Core Ops, SparseCore 0:
  58.6 42.0 all-gather.10
  102.8 32.6 all-gather.14
  137.0 34.4 all-gather.12
  179.1 194.2 all-gather.22
  374.8 32.5 all-gather.16
  409.4 34.4 all-gather.20
  445.4 34.4 all-gather.18
  487.9 149.6 all-gather.24
